TPU v7x, 128 devices: a whole 4x4x4 slice. The times are simulated.
128 devices in a mesh: sp: 32 (over z, y, core), tp: 4 (over x).
Axes of the slice: x: 4, y: 4, z: 4, core: 2. Of those that a mesh axis runs over, the one named last changes fastest.
Arguments:
- tokens: bfloat16 [8192, 4096], P(('sp', 'tp')), may hold values from -6 to 6, as said below
- query_one: bfloat16 [4096, 1024], P('sp', 'tp'), may hold values from -0.125 to 0.125
- query_two: bfloat16 [4096, 1024], P('sp', 'tp'), may hold values from -0.125 to 0.125
- key_one: bfloat16 [4096, 1024], P('sp', 'tp'), may hold values from -0.125 to 0.125
- key_two: bfloat16 [4096, 1024], P('sp', 'tp'), may hold values from -0.125 to 0.125
- value_weight: bfloat16 [4096, 2048], P('sp', 'tp'), may hold values from -0.09375 to 0.09375
- out_weight: bfloat16 [2048, 4096], P('tp', 'sp'), may hold values from -0.125 to 0.125
- lambdas: float32 [8], P('tp'), may hold values from 0.3 to 0.8
- head_gain: float32 [256], replicated, may hold values from 0.1 to 1.9
Outputs:
- layer_out: bfloat16 [8192, 4096], P(('sp', 'tp'))
Inputs may be any that keep to these rules, and one draw needn't show every extreme that they name: `tokens`: the features' mean changes between 16 equal spans of the sequence.
All inputs are finite; a program needn't handle non-finite values.
Results may differ from a plain program's by a relative error of at most 0.013.
The roundings to bfloat16 on the way count: a program that leaves them out, or rounds other values in their place, can miss the bound.
Values may be sent and summed in bfloat16 or wider, within the bound.
A program may use at most 128 MiB of HBM per device.

v0:
```python
import jax
import jax.numpy as jnp
import numpy as np
from jax import lax
from jax.experimental import pallas as pl
from jax.experimental.pallas import tpu as pltpu
from jax.sharding import Mesh, PartitionSpec as P

QK = 128
V = 256
ROPE_BASE = 500000.0
EPS_NORM = 0.02
LOG2E = 1.4426950408889634
ROWS = 512
BF = jnp.bfloat16
F32 = jnp.float32
MESH = pl.DeviceIdType.MESH
AXES = ("z", "y", "core", "x")


def dot(a, b, dims=(((1,), (0,)), ((), ()))):
    return lax.dot_general(a, b, dims, preferred_element_type=F32)


class Links:
    def __init__(self):
        self.at = {a: lax.axis_index(a) for a in AXES}
        self.sent = []

    def peer(self, axis, step):
        n = 2 if axis == "core" else 4
        return {axis: lax.rem(self.at[axis] + (step + n), n)}

    def send(self, views, axis, step):
        def copy():
            return pltpu.make_async_remote_copy(*views(), device_id=self.peer(axis, step), device_id_type=MESH)

        copy().start()
        self.sent.append(copy)

    def arrived(self, view, ssem, rsem, axis, step):
        pltpu.make_async_remote_copy(view, view, ssem, rsem, device_id=self.peer(axis, step), device_id_type=MESH).wait_recv()

    def drain(self):
        for copy in self.sent:
            copy().wait_send()


NEAR = (0, -1, 1, 2)


class TorusGather:
    def __init__(self, links, piece, ssem, rsem):
        self.links, self.piece, self.ssem, self.rsem = links, piece, ssem, rsem

    def ref(self, half, dp, ds, sub=None):
        dz, dy = (ds, dp) if half == 0 else (dp, ds)
        return self.piece(dz, dy, half, sub)

    def axes(self, half):
        return ("y", "z") if half == 0 else ("z", "y")

    def out(self, half, key, dp, ds, sub, second, step):
        k = half * 20 + key
        def views():
            view = self.ref(half, dp, ds, sub)
            return view, view, self.ssem.at[k], self.rsem.at[k]

        self.links.send(views, self.axes(half)[second], step)

    def wait(self, half, key, dp, ds, sub, second, step):
        k = half * 20 + key
        self.links.arrived(self.ref(half, dp, ds, sub), self.ssem.at[k], self.rsem.at[k], self.axes(half)[second], step)

    def spread(self, half, dp):
        i = NEAR.index(dp)
        self.out(half, 4 + 4 * i, dp, 0, None, 1, 1)
        self.out(half, 5 + 4 * i, dp, 0, None, 1, -1)

    def begin(self):
        for half in (0, 1):
            self.out(half, 0, 0, 0, None, 0, 1)
            self.out(half, 1, 0, 0, None, 0, -1)
        for half in (0, 1):
            self.spread(half, 0)

    def first(self):
        for half in (0, 1):
            self.wait(half, 0, -1, 0, None, 0, -1)
            self.out(half, 2, -1, 0, 0, 0, 1)
            self.wait(half, 1, 1, 0, None, 0, 1)
            self.out(half, 3, 1, 0, 1, 0, -1)
        for half in (0, 1):
            self.spread(half, -1)
            self.spread(half, 1)

    def opposite(self):
        for half in (0, 1):
            self.wait(half, 2, 2, 0, 0, 0, -1)
            self.wait(half, 3, 2, 0, 1, 0, 1)
            self.spread(half, 2)

    def second(self, dp, step):
        i = NEAR.index(dp)
        for half in (0, 1):
            if step < 0:
                self.wait(half, 4 + 4 * i, dp, -1, None, 1, -1)
                self.out(half, 6 + 4 * i, dp, -1, 0, 1, 1)
            else:
                self.wait(half, 5 + 4 * i, dp, 1, None, 1, 1)
                self.out(half, 7 + 4 * i, dp, 1, 1, 1, -1)

    def third(self, dp):
        i = NEAR.index(dp)
        for half in (0, 1):
            self.wait(half, 6 + 4 * i, dp, 2, 0, 1, -1)
            self.wait(half, 7 + 4 * i, dp, 2, 1, 1, 1)

    def steps(self):
        second, third = self.second, self.third
        return [
            ([self.first, lambda: second(0, -1)], (-1, 0)),
            ([], (0, -1)),
            ([lambda: second(0, 1)], (1, 0)),
            ([], (0, 1)),
            ([self.opposite, lambda: second(-1, -1)], (-1, -1)),
            ([lambda: second(-1, 1), lambda: second(1, -1)], (1, -1)),
            ([], (-1, 1)),
            ([lambda: second(1, 1)], (1, 1)),
            ([lambda: third(0)], (0, 2)),
            ([], (2, 0)),
            ([lambda: second(2, -1), lambda: second(2, 1), lambda: third(-1)], (-1, 2)),
            ([], (2, -1)),
            ([lambda: third(1)], (1, 2)),
            ([], (2, 1)),
            ([lambda: third(2)], (2, 2)),
        ]


def pick(t, values):
    result = values[0]
    for k in range(1, len(values)):
        result = jnp.where(t == k, values[k], result)
    return result


def on_step(t, k, actions):
    if actions:

        @pl.when(t == k)
        def _():
            for action in actions:
                action()


def layer_kernel(
    tok, wq1, wq2, wk1, wk2, wv, wo, lam, gain, inverse, out, cos, sin,
    tbuf, wbuf, proj, qbuf, kvbuf, obuf, abuf, acc, top, tot,
    fsend, frecv, nsend, nrecv, osend, orecv, mine,
    lsem, wss, wrs, kss, krs, oss, ors, tss, trs, sss, srs, xss, xrs,
):
    links = Links()
    z, y, core, x = [links.at[a] for a in AXES]
    chip = z * 4 + y
    scale = QK ** (-0.5)

    def slot(dz, dy):
        return lax.rem(z + (dz + 4), 4) * 4 + lax.rem(y + (dy + 4), 4)

    def plain(src, dst, ssem, rsem, axis, step):
        links.send(lambda: (src, dst, ssem, rsem), axis, step)

    barrier = pltpu.get_barrier_semaphore()
    peers = [("core", 1)] + [(a, s) for a in ("x", "y", "z") for s in (1, -1)]
    for axis, step in peers:
        pl.semaphore_signal(barrier, inc=1, device_id=links.peer(axis, step), device_id_type=MESH)
    pl.semaphore_wait(barrier, len(peers))

    own_rows = pl.ds(pl.multiple_of(chip * 256 + core * 128, 128), 128)
    sib_rows = pl.ds(pl.multiple_of(chip * 256 + (1 - core) * 128, 128), 128)
    local = []
    column = 0
    cuts = []
    for i, (w, width) in enumerate(((wq1, QK), (wq2, QK), (wk1, QK), (wk2, QK), (wv, V))):
        here = w.at[:, pl.ds(pl.multiple_of(core * width, 128), width)]
        there = w.at[:, pl.ds(pl.multiple_of((1 - core) * width, 128), width)]
        cols = pl.ds(column, width)
        cuts.append(cols)
        plain(there, wbuf.at[own_rows, cols], sss.at[i], srs.at[i], "core", 1)
        local.append(pltpu.make_async_copy(here, wbuf.at[own_rows, cols], lsem.at[i]))
        local[-1].start()
        column += width

    def trows(c, dx, sub=None):
        start = c * 256 + lax.rem(x + (dx + 4), 4) * 64
        if sub is None:
            return tbuf.at[pl.ds(pl.multiple_of(start, 64), 64), :]
        return tbuf.at[pl.ds(pl.multiple_of(start + sub * 32, 32), 32), :]

    own_tokens = pltpu.make_async_copy(tok, trows(core, 0), lsem.at[5])
    own_tokens.start()
    plain(tok, trows(core, 0), tss.at[0], trs.at[0], "x", 1)
    plain(tok, trows(core, 0), tss.at[1], trs.at[1], "x", -1)
    plain(tok, trows(core, 0), sss.at[5], srs.at[5], "core", 1)
    own_columns = pl.ds(pl.multiple_of(chip * 128, 128), 128)
    own_out = pltpu.make_async_copy(wo, obuf.at[:, own_columns], lsem.at[6])
    own_out.start()

    for i in range(5):
        local[i].wait()
        links.arrived(wbuf.at[sib_rows, cuts[i]], sss.at[i], srs.at[i], "core", 1)

    def wpiece(dz, dy, half, sub):
        start = slot(dz, dy) * 256 + half * 128
        if sub is None:
            return wbuf.at[pl.ds(pl.multiple_of(start, 128), 128), :]
        return wbuf.at[pl.ds(pl.multiple_of(start + sub * 64, 64), 64), :]

    weights = TorusGather(links, wpiece, wss, wrs)
    weights.begin()

    def pass_on(dx, sub, ssem, rsem, i, axis, step):
        def views():
            return trows(core, dx, sub), trows(core, dx, sub), ssem.at[i], rsem.at[i]

        links.send(views, axis, step)

    def near_tokens():
        links.arrived(trows(core, -1), tss.at[0], trs.at[0], "x", -1)
        pass_on(-1, 0, tss, trs, 2, "x", 1)
        pass_on(-1, None, sss, srs, 6, "core", 1)
        links.arrived(trows(core, 1), tss.at[1], trs.at[1], "x", 1)
        pass_on(1, 1, tss, trs, 3, "x", -1)
        pass_on(1, None, sss, srs, 7, "core", 1)

    def far_tokens():
        links.arrived(trows(core, 2, 0), tss.at[2], trs.at[2], "x", -1)
        links.arrived(trows(core, 2, 1), tss.at[3], trs.at[3], "x", 1)
        pass_on(2, None, sss, srs, 8, "core", 1)
        own_tokens.wait()
        for i, dx in ((5, 0), (6, -1), (7, 1), (8, 2)):
            links.arrived(trows(1 - core, dx), sss.at[i], srs.at[i], "core", 1)

    steps = weights.steps()
    early = [action for actions, _ in steps[:5] for action in actions] + [near_tokens]
    early += [action for actions, _ in steps[5:8] for action in actions] + [far_tokens]
    dzs = [0] + [d for _, (d, _) in steps]
    dys = [0] + [d for _, (_, d) in steps]
    proj[...] = jnp.zeros_like(proj)
    half_dim = QK // 2
    position = chip * ROWS + lax.broadcasted_iota(jnp.int32, (ROWS, half_dim), 0)
    angle = position.astype(F32) * inverse[...]
    cos_part, sin_part = jnp.cos(angle), jnp.sin(angle)
    cos[:, :half_dim] = cos_part
    cos[:, half_dim:] = cos_part
    sin[:, :half_dim] = -sin_part
    sin[:, half_dim:] = sin_part

    @pl.loop(0, 16)
    def _(t):
        on_step(t, 0, early)
        for k in range(9, 16):
            on_step(t, k, steps[k - 1][0])
        depth = pl.ds(pl.multiple_of(slot(pick(t, dzs), pick(t, dys)) * 256, 256), 256)
        proj[...] += dot(tbuf[:, depth], wbuf[depth, :])


    def opiece(dz, dy, half, sub):
        cols = pl.ds(pl.multiple_of(slot(dz, dy) * 128, 128), 128)
        if sub is None:
            return obuf.at[pl.ds(half * 256, 256), cols]
        return obuf.at[pl.ds(half * 256 + sub * 128, 128), cols]

    own_out.wait()
    columns = TorusGather(links, opiece, oss, ors)
    columns.begin()

    def turned(i):
        v = proj[:, i * QK : (i + 1) * QK]
        swapped = jnp.concatenate([v[:, QK // 2 :], v[:, : QK // 2]], axis=1)
        return (v * cos[...] + swapped * sin[...]).astype(BF)

    own_keys = pl.ds(pl.multiple_of(chip * ROWS, ROWS), ROWS)
    kvbuf[own_keys, 0:QK] = turned(2)
    kvbuf[own_keys, QK : 2 * QK] = turned(3)
    kvbuf[own_keys, 2 * QK :] = proj[:, 4 * QK :].astype(BF)

    def kpiece(dz, dy, half, sub):
        start = slot(dz, dy) * ROWS + half * 256
        if sub is None:
            return kvbuf.at[pl.ds(pl.multiple_of(start, 256), 256), :]
        return kvbuf.at[pl.ds(pl.multiple_of(start + sub * 128, 128), 128), :]

    keys = TorusGather(links, kpiece, kss, krs)
    keys.begin()
    qbuf[0] = turned(0)
    qbuf[1] = turned(1)

    log_scale = scale * LOG2E

    def attend(index, diagonal):
        span = pl.ds(pl.multiple_of(index * ROWS, ROWS), ROWS)
        v = kvbuf[span, 2 * QK :]
        for r in range(2):
            rows = pl.ds(r * 256, 256)
            for a in range(2):
                s = dot(qbuf[a, rows], kvbuf[span, a * QK : (a + 1) * QK], (((1,), (1,)), ((), ())))
                if diagonal:
                    row_ids = r * 256 + lax.broadcasted_iota(jnp.int32, s.shape, 0)
                    s = jnp.where(lax.broadcasted_iota(jnp.int32, s.shape, 1) <= row_ids, s, -1e30)
                parts = [s[:, k * 128 : (k + 1) * 128] for k in range(4)]
                high = jnp.maximum(jnp.maximum(parts[0], parts[1]), jnp.maximum(parts[2], parts[3]))
                high = jnp.max(high, axis=1, keepdims=True) * log_scale
                if diagonal:
                    new = high
                else:
                    old = top[a, rows][:, :1]
                    new = jnp.maximum(old, high)
                e = jnp.exp2(s * log_scale - new)
                total = (e[:, 0:128] + e[:, 128:256]) + (e[:, 256:384] + e[:, 384:512])
                weighted = dot(e.astype(BF), v)
                if diagonal:
                    tot[a, rows] = total
                    acc[a, rows] = weighted
                else:
                    fade = jnp.exp2(old - new)
                    tot[a, rows] = tot[a, rows] * fade + total
                    acc[a, rows] = acc[a, rows] * fade + weighted
                top[a, rows] = jnp.broadcast_to(new, (256, 128))

    attend(chip, True)

    columns.first()
    for dp in (0,):
        columns.second(dp, -1)
        columns.second(dp, 1)
    columns.opposite()
    for dp in (-1, 1, 2):
        columns.second(dp, -1)
        columns.second(dp, 1)
    for dp in NEAR:
        columns.third(dp)
    ksteps = keys.steps()

    @pl.loop(0, 15)
    def _(t):
        for k in range(15):
            on_step(t, k, ksteps[k][0])
        index = slot(pick(t, dzs[1:]), pick(t, dys[1:]))

        @pl.when(index < chip)
        def _():
            attend(index, False)

    o1 = acc[0] / jnp.sum(tot[0], axis=1, keepdims=True)
    o2 = acc[1] / jnp.sum(tot[1], axis=1, keepdims=True)
    mixed = o1 - lam[core] * o2
    norm = lax.rsqrt(jnp.mean(mixed * mixed, axis=1, keepdims=True) + EPS_NORM)
    mine[...] = (mixed * norm * gain[...]).astype(BF)
    plain(mine, abuf.at[core], xss.at[0], xrs.at[0], "core", 1)
    keep = pltpu.make_async_copy(mine, abuf.at[core], lsem.at[7])
    keep.start()
    keep.wait()
    links.arrived(abuf.at[1 - core], xss.at[0], xrs.at[0], "core", 1)

    def partial(dx, r):
        start = r * 256 + lax.rem(x + (dx + 4), 4) * 64
        rows = pl.ds(pl.multiple_of(start, 64), 64)
        return dot(abuf[0, rows, :], obuf[0:256, :]) + dot(abuf[1, rows, :], obuf[256:512, :])

    for r in (0, 1):
        fsend[r] = partial(2, r).astype(BF)
        step = 1 if r == 0 else -1
        plain(fsend.at[r], frecv.at[r], xss.at[1 + r], xrs.at[1 + r], "x", step)
    for r in (0, 1):
        step = -1 if r == 0 else 1
        nsend[r, r] = partial(step, r).astype(BF)
        plain(nsend.at[r, r], nrecv.at[r, r], xss.at[3 + r], xrs.at[3 + r], "x", step)
    for r in (0, 1):
        step = 1 if r == 0 else -1
        term = partial(step, r)
        links.arrived(frecv.at[r], xss.at[1 + r], xrs.at[1 + r], "x", -step)
        nsend[1 - r, r] = (term + frecv[r].astype(F32)).astype(BF)
        plain(nsend.at[1 - r, r], nrecv.at[1 - r, r], xss.at[5 + r], xrs.at[5 + r], "x", step)
    sums = [partial(0, 0), partial(0, 1)]
    for r in (0, 1):
        step = -1 if r == 0 else 1
        links.arrived(nrecv.at[r, r], xss.at[3 + r], xrs.at[3 + r], "x", -step)
        sums[r] = sums[r] + nrecv[r, r].astype(F32)
    for r in (0, 1):
        step = 1 if r == 0 else -1
        links.arrived(nrecv.at[1 - r, r], xss.at[5 + r], xrs.at[5 + r], "x", -step)
        osend[r] = (sums[r] + nrecv[1 - r, r].astype(F32)).astype(BF)
    plain(osend.at[1 - core], orecv, xss.at[7], xrs.at[7], "core", 1)
    links.arrived(orecv, xss.at[7], xrs.at[7], "core", 1)
    own = osend[core]
    other = orecv[...]
    low = jnp.where(core == 0, own, other)
    high = jnp.where(core == 0, other, own)
    for k in range(16):
        out[:, k * 256 : k * 256 + 128] = low[:, k * 128 : (k + 1) * 128]
        out[:, k * 256 + 128 : k * 256 + 256] = high[:, k * 128 : (k + 1) * 128]
    links.drain()


def on_device(tokens, query_one, query_two, key_one, key_two, value_weight, out_weight, lambdas, head_gain):
    inverse = 1.0 / np.float32(ROPE_BASE) ** (np.arange(0, QK, 2, dtype=np.float32) / np.float32(QK))
    vm = pl.BlockSpec(memory_space=pltpu.VMEM)
    dma = pltpu.SemaphoreType.DMA
    return pl.pallas_call(
        layer_kernel,
        out_shape=jax.ShapeDtypeStruct((64, 4096), BF),
        in_specs=[vm] * 7 + [pl.BlockSpec(memory_space=pltpu.SMEM)] + [vm] * 2,
        out_specs=vm,
        scratch_shapes=[
            pltpu.VMEM((ROWS, QK), F32),
            pltpu.VMEM((ROWS, QK), F32),
            pltpu.VMEM((512, 4096), BF),
            pltpu.VMEM((4096, 768), BF),
            pltpu.VMEM((ROWS, 768), F32),
            pltpu.VMEM((2, ROWS, QK), BF),
            pltpu.VMEM((8192, 512), BF),
            pltpu.VMEM((512, 2048), BF),
            pltpu.VMEM((2, ROWS, V), BF),
            pltpu.VMEM((2, ROWS, V), F32),
            pltpu.VMEM((2, ROWS, 128), F32),
            pltpu.VMEM((2, ROWS, 128), F32),
            pltpu.VMEM((2, 64, 2048), BF),
            pltpu.VMEM((2, 64, 2048), BF),
            pltpu.VMEM((2, 2, 64, 2048), BF),
            pltpu.VMEM((2, 2, 64, 2048), BF),
            pltpu.VMEM((2, 64, 2048), BF),
            pltpu.VMEM((64, 2048), BF),
            pltpu.VMEM((ROWS, V), BF),
            dma((8,)),
            dma((40,)), dma((40,)),
            dma((40,)), dma((40,)),
            dma((40,)), dma((40,)),
            dma((4,)), dma((4,)),
            dma((9,)), dma((9,)),
            dma((8,)), dma((8,)),
        ],
        compiler_params=pltpu.CompilerParams(
            collective_id=0, has_side_effects=True, vmem_limit_bytes=60 * 1024 * 1024
        ),
    )(tokens, query_one, query_two, key_one, key_two, value_weight, out_weight, lambdas, head_gain[None], jnp.asarray(inverse[None], F32))


def solution(mesh):
    fine = Mesh(mesh.devices.reshape(4, 4, 2, 4), AXES)
    sp = ("z", "y", "core")
    in_specs = (
        P((*sp, "x"), None),
        P(sp, "x"),
        P(sp, "x"),
        P(sp, "x"),
        P(sp, "x"),
        P(sp, "x"),
        P("x", sp),
        P("x"),
        P(),
    )
    return jax.shard_map(on_device, mesh=fine, in_specs=in_specs, out_specs=P((*sp, "x"), None), check_vma=False)
```

profile of v0, /device:TPU:1, one launch (start us, length us, event | category | flops | bytes accessed | tf_op | source)
XLA Modules:
  0.0 132.1 jit_solution(3184405220027204691)
XLA Ops:
  0.0 130.2 %shard_map.100 = bf16[64,4096]{1,0:T(8,128)(2,1)} custom-call(bf16[64,4096]{1,0:T(8,128)(2,1)} %tok.1, bf16[128,256]{1,0:T(8,128)(2,1)} %wq1.1, bf16[128,256]{1,0:T(8,128)(2,1)} %wq2.1, bf16[128,256]{1,0:T(8,128)(2,1)} %wk1.1, bf16[128,256]{1,0:T(8,128)(2,1)} %wk2.1, bf16[128,512]{1,0:T(8,128)(2,1)} %wv.1, bf16[512,128]{1,0:T(8,128)(2,1)} %wo.1, f32[2]{0:T(128)} %lam.1, ...), custom_call_target="tpu_custom_call" | custom-call | tf_op jit(solution)/shard_map/pallas_call | solution.py:410
  130.2 1.9 %copy.12 = bf16[64,4096]{1,0:T(8,128)(2,1)} copy(bf16[64,4096]{1,0:T(8,128)(2,1)} %shard_map.100) | data formatting | bytes 1048576
where the time goes:
time: 135 us; the launch traced here: 132 us
  Pallas kernels  130 us (96%)
  local copies, waits for them, and re-layouts  1.87 us (1%)
    pallas_call x1, Pallas kernels, on_device(): pl.pallas_call(layer_kernel, out_shape=jax.ShapeDtypeStruct((64, 4096), B...  130 us

commit v1 on v0

v1 whole, which is shorter than its diff:
```python
import jax
import jax.numpy as jnp
import numpy as np
from jax import lax
from jax.experimental import pallas as pl
from jax.experimental.pallas import tpu as pltpu
from jax.sharding import Mesh, PartitionSpec as P

QK = 128
V = 256
ROPE_BASE = 500000.0
EPS_NORM = 0.02
LOG2E = 1.4426950408889634
ROWS = 512
BF = jnp.bfloat16
F32 = jnp.float32
MESH = pl.DeviceIdType.MESH
AXES = ("z", "y", "core", "x")
NEAR = (0, -1, 1, 2)


def dot(a, b, dims=(((1,), (0,)), ((), ()))):
    return lax.dot_general(a, b, dims, preferred_element_type=F32)


class Links:
    def __init__(self):
        self.z, self.y, self.core, self.x = [lax.axis_index(a) for a in AXES]
        self.u = self.y * (1 - self.core) + self.x * self.core
        self.w = self.x * (1 - self.core) + self.y * self.core
        self.sent = []

    def peer(self, axis, step):
        if axis == "core":
            return {"core": 1 - self.core}
        if axis == "even":
            return {"core": 0}
        if axis == "odd":
            return {"y": self.x, "core": 1, "x": self.y}
        if axis == "z":
            return {"z": lax.rem(self.z + (step + 4), 4)}
        along = self.core if axis == "u" else 1 - self.core
        return {"y": lax.rem(self.y + (4 + step * (1 - along)), 4), "x": lax.rem(self.x + (4 + step * along), 4)}

    def send(self, views, axis, step, only=None):
        def copy():
            return pltpu.make_async_remote_copy(*views(), device_id=self.peer(axis, step), device_id_type=MESH)

        if only is None:
            copy().start()
        else:
            pl.when(only)(lambda: copy().start())
        self.sent.append((copy, only))

    def arrived(self, view, ssem, rsem):
        pltpu.make_async_remote_copy(view, view, ssem, rsem, device_id=self.peer("core", 1), device_id_type=MESH).wait_recv()

    def drain(self):
        for copy, only in self.sent:
            if only is None:
                copy().wait_send()
            else:
                pl.when(only)(lambda copy=copy: copy().wait_send())


class TorusGather:
    def __init__(self, links, piece, ssem, rsem):
        self.links, self.piece, self.ssem, self.rsem = links, piece, ssem, rsem

    def ref(self, part, dp, ds, sub=None):
        dz, du = (ds, dp) if part == 0 else (dp, ds)
        return self.piece(dz, du, part, sub)

    def axis(self, part, second):
        return ("u", "z")[part ^ second]

    def out(self, part, key, dp, ds, sub, second, step):
        k = part * 20 + key

        def views():
            view = self.ref(part, dp, ds, sub)
            return view, view, self.ssem.at[k], self.rsem.at[k]

        self.links.send(views, self.axis(part, second), step)

    def wait(self, part, key, dp, ds, sub):
        k = part * 20 + key
        self.links.arrived(self.ref(part, dp, ds, sub), self.ssem.at[k], self.rsem.at[k])

    def spread(self, part, dp):
        i = NEAR.index(dp)
        self.out(part, 4 + 4 * i, dp, 0, None, 1, 1)
        self.out(part, 5 + 4 * i, dp, 0, None, 1, -1)

    def begin(self):
        for part in (0, 1):
            self.out(part, 0, 0, 0, None, 0, 1)
            self.out(part, 1, 0, 0, None, 0, -1)
        for part in (0, 1):
            self.spread(part, 0)

    def first(self):
        for part in (0, 1):
            self.wait(part, 0, -1, 0, None)
            self.out(part, 2, -1, 0, 0, 0, 1)
            self.wait(part, 1, 1, 0, None)
            self.out(part, 3, 1, 0, 1, 0, -1)
        for part in (0, 1):
            self.spread(part, -1)
            self.spread(part, 1)

    def opposite(self):
        for part in (0, 1):
            self.wait(part, 2, 2, 0, 0)
            self.wait(part, 3, 2, 0, 1)
            self.spread(part, 2)

    def second(self, dp, step):
        i = NEAR.index(dp)
        for part in (0, 1):
            if step < 0:
                self.wait(part, 4 + 4 * i, dp, -1, None)
                self.out(part, 6 + 4 * i, dp, -1, 0, 1, 1)
            else:
                self.wait(part, 5 + 4 * i, dp, 1, None)
                self.out(part, 7 + 4 * i, dp, 1, 1, 1, -1)

    def third(self, dp):
        i = NEAR.index(dp)
        for part in (0, 1):
            self.wait(part, 6 + 4 * i, dp, 2, 0)
            self.wait(part, 7 + 4 * i, dp, 2, 1)

    def steps(self):
        second, third = self.second, self.third
        return [
            ([self.first, lambda: second(0, -1)], (-1, 0)),
            ([], (0, -1)),
            ([lambda: second(0, 1)], (1, 0)),
            ([], (0, 1)),
            ([self.opposite, lambda: second(-1, -1)], (-1, -1)),
            ([lambda: second(-1, 1), lambda: second(1, -1)], (1, -1)),
            ([], (-1, 1)),
            ([lambda: second(1, 1)], (1, 1)),
            ([lambda: third(0)], (0, 2)),
            ([], (2, 0)),
            ([lambda: second(2, -1), lambda: second(2, 1), lambda: third(-1)], (-1, 2)),
            ([], (2, -1)),
            ([lambda: third(1)], (1, 2)),
            ([], (2, 1)),
            ([lambda: third(2)], (2, 2)),
        ]


def pick(t, values):
    result = values[0]
    for k in range(1, len(values)):
        result = jnp.where(t == k, values[k], result)
    return result


def on_step(t, k, actions):
    if actions:

        @pl.when(t == k)
        def _():
            for action in actions:
                action()


def window(start, size):
    return pl.ds(pl.multiple_of(start, size), size)


def layer_kernel(
    tok, wq1, wq2, wk1, wk2, wv, wo, lam, gain, inverse, out, cos, sin,
    tbuf, wbuf, proj, qbuf, kvbuf, obuf, acc, top, tot,
    fsend, frecv, nsend, nrecv, keep, sums, osend, orecv, mine, lown, lrecv,
    lsem, wss, wrs, kss, krs, oss, ors, tss, trs, sss, srs, xss, xrs,
):
    links = Links()
    z, y, core, x, u, w = links.z, links.y, links.core, links.x, links.u, links.w
    chip = z * 4 + y
    place = z * 4 + u
    log_scale = QK ** (-0.5) * LOG2E

    def slot(dz, du):
        return lax.rem(z + (dz + 4), 4) * 4 + lax.rem(u + (du + 4), 4)

    def plain(src, dst, ssem, rsem, axis, step=1, only=None):
        links.send(lambda: (src, dst, ssem, rsem), axis, step, only)

    barrier = pltpu.get_barrier_semaphore()
    for axis, step in [("core", 1)] + [(a, s) for a in ("u", "w", "z") for s in (1, -1)]:
        pl.semaphore_signal(barrier, inc=1, device_id=links.peer(axis, step), device_id_type=MESH)
    crossed = x != y

    @pl.when(jnp.logical_and(core == 1, crossed))
    def _():
        for other in (0, 1):
            pl.semaphore_signal(barrier, inc=1, device_id={"y": x, "core": other, "x": y}, device_id_type=MESH)

    pl.semaphore_wait(barrier, 7 + jnp.where(crossed, 1, 0))

    def trows(dw, c):
        return tbuf.at[window(NEAR.index(dw) * 128 + c * 64, 64), :]

    own_tokens = pltpu.make_async_copy(tok, trows(0, core), lsem.at[0])
    own_tokens.start()

    own_rows = window(chip * 256 + core * 128, 128)
    items = []
    column = 0
    for ref, width in ((wq1, QK), (wq2, QK), (wk1, QK), (wk2, QK), (wv, V)):
        cols = pl.ds(column, width)
        items.append((ref.at[:, pl.ds(0, width)], ref.at[:, pl.ds(width, width)], wbuf.at[own_rows, cols]))
        column += width
    items.append((wo.at[pl.ds(0, 256), :], wo.at[pl.ds(256, 256), :], obuf.at[:, window((chip * 2 + core) * 128, 128)]))
    stays = jnp.logical_and(core == 1, x == y)
    leaves = jnp.logical_not(stays)

    def hand_over(which):
        for i in which:
            even, odd, dst = items[i]
            k = core * 6 + i
            plain(odd, dst, sss.at[6 + i], srs.at[k], "odd", only=leaves)
            pl.when(stays)(lambda: pltpu.make_async_copy(odd, dst, srs.at[k]).start())
            plain(even, dst, sss.at[i], srs.at[k], "even", only=core == 1)
            pl.when(core == 0)(lambda: pltpu.make_async_copy(even, dst, srs.at[k]).start())

    hand_over(range(5))
    plain(tok, tbuf.at[window(core * 64, 64), :], tss.at[6], trs.at[6], "core")
    plain(tok, tbuf.at[window(NEAR.index(-1) * 128 + core * 64, 64), :], tss.at[core], trs.at[core], "w", 1)
    plain(tok, tbuf.at[window(NEAR.index(1) * 128 + core * 64, 64), :], tss.at[2 + core], trs.at[2 + core], "w", -1)
    hand_over([5])

    for c in (0, 1):
        column = 0
        for i, width in enumerate((QK, QK, QK, QK, V)):
            view = wbuf.at[window(place * 256 + c * 128, 128), pl.ds(column, width)]
            links.arrived(view, sss.at[i], srs.at[c * 6 + i])
            column += width

    def wpiece(dz, du, part, sub):
        start = slot(dz, du) * 256 + part * 128
        if sub is None:
            return wbuf.at[window(start, 128), :]
        return wbuf.at[window(start + sub * 64, 64), :]

    weights = TorusGather(links, wpiece, wss, wrs)
    weights.begin()

    links.arrived(trows(0, 1 - core), tss.at[6], trs.at[6])
    sibling = trows(0, 1 - core)
    plain(sibling, tbuf.at[window(NEAR.index(-1) * 128 + (1 - core) * 64, 64), :], tss.at[1 - core], trs.at[1 - core], "w", 1)
    plain(sibling, tbuf.at[window(NEAR.index(1) * 128 + (1 - core) * 64, 64), :], tss.at[3 - core], trs.at[3 - core], "w", -1)

    lown[...] = jnp.full((8, 128), jnp.where(core == 0, lam[0], lam[1]), F32)

    def pass_on(dw, c, k, step):
        links.send(lambda: (trows(dw, c), trows(2, c), tss.at[k], trs.at[k]), "w", step)

    def near_tokens():
        for c in (0, 1):
            links.arrived(trows(-1, c), tss.at[c], trs.at[c])
        pass_on(-1, 0, 4, 1)
        for c in (0, 1):
            links.arrived(trows(1, c), tss.at[2 + c], trs.at[2 + c])
        pass_on(1, 1, 5, -1)
        own_tokens.wait()

    def far_tokens():
        for c in (0, 1):
            links.arrived(trows(2, c), tss.at[4 + c], trs.at[4 + c])

    def positions(ids, at_u):
        rel = ids // 128
        step = jnp.where(rel == 1, 3, jnp.where(rel == 2, 1, jnp.where(rel == 3, 2, 0)))
        along = (w + step) & 3
        return z * 2048 + at_u * (512 - 448 * core) + along * (64 + 448 * core) + ((ids // 64) & 1) * 256 + (ids & 63)

    half_dim = QK // 2
    position = positions(lax.broadcasted_iota(jnp.int32, (ROWS, half_dim), 0), u)
    angle = position.astype(F32) * inverse[...]
    cos_part, sin_part = jnp.cos(angle), jnp.sin(angle)
    cos[:, :half_dim] = cos_part
    cos[:, half_dim:] = cos_part
    sin[:, :half_dim] = -sin_part
    sin[:, half_dim:] = sin_part
    proj[...] = jnp.zeros_like(proj)

    steps = weights.steps()
    early = [action for actions, _ in steps[:8] for action in actions] + [near_tokens]
    dzs = [0] + [d for _, (d, _) in steps]
    dus = [0] + [d for _, (_, d) in steps]

    @pl.loop(0, 16)
    def _(t):
        on_step(t, 0, early)
        on_step(t, 5, [lambda: weights.third(0), lambda: weights.second(2, -1), lambda: weights.second(2, 1)])
        on_step(t, 11, [lambda: weights.third(-1)])
        on_step(t, 13, [lambda: weights.third(1)])
        on_step(t, 15, [lambda: weights.third(2)])
        depth = window(slot(pick(t, dzs), pick(t, dus)) * 256, 256)
        proj[0:384, :] += dot(tbuf[0:384, depth], wbuf[depth, :])

    def opiece(dz, du, part, sub):
        cols = window(slot(dz, du) * 256, 256)
        start, size = ((0, 64), (64, 192))[part]
        if sub is None:
            return obuf.at[pl.ds(start, size), cols]
        return obuf.at[pl.ds(start + sub * (size // 2), size // 2), cols]

    for c in (0, 1):
        links.arrived(obuf.at[:, window((place * 2 + c) * 128, 128)], sss.at[5], srs.at[c * 6 + 5])
    columns = TorusGather(links, opiece, oss, ors)
    columns.begin()
    far_tokens()
    proj[384:512, :] = dot(tbuf[384:512, :], wbuf[...])

    def turned(i):
        v = proj[:, i * QK : (i + 1) * QK]
        swapped = jnp.concatenate([v[:, QK // 2 :], v[:, : QK // 2]], axis=1)
        return (v * cos[...] + swapped * sin[...]).astype(BF)

    own_keys = window(place * ROWS, ROWS)
    kvbuf[own_keys, 0:QK] = turned(2)
    kvbuf[own_keys, QK : 2 * QK] = turned(3)
    kvbuf[own_keys, 2 * QK :] = proj[:, 4 * QK :].astype(BF)

    def kpiece(dz, du, part, sub):
        start, size = ((0, 128), (128, 384))[part]
        base = slot(dz, du) * ROWS + start
        if sub is None:
            return kvbuf.at[pl.ds(pl.multiple_of(base, 128), size), :]
        return kvbuf.at[pl.ds(pl.multiple_of(base + sub * (size // 2), 64), size // 2), :]

    keys = TorusGather(links, kpiece, kss, krs)
    keys.begin()
    crosses = jnp.logical_and(core == 1, crossed)
    plain(lown, lrecv, xss.at[0], xrs.at[0], "odd", only=crosses)
    pl.when(jnp.logical_not(crosses))(lambda: pltpu.make_async_copy(lown, lrecv, xrs.at[0]).start())
    qbuf[0] = turned(0)
    qbuf[1] = turned(1)

    def attend(index, at_u, masked, opening):
        span = window(index * ROWS, ROWS)
        v = kvbuf[span, 2 * QK :]
        for r in range(2):
            rows = pl.ds(r * 256, 256)
            if masked:
                query_at = positions(r * 256 + lax.broadcasted_iota(jnp.int32, (256, ROWS), 0), u)
                key_at = positions(lax.broadcasted_iota(jnp.int32, (256, ROWS), 1), at_u)
                allowed = key_at <= query_at
            for a in range(2):
                s = dot(qbuf[a, rows], kvbuf[span, a * QK : (a + 1) * QK], (((1,), (1,)), ((), ())))
                if masked:
                    s = jnp.where(allowed, s, -1e30)
                parts = [s[:, k * 128 : (k + 1) * 128] for k in range(4)]
                high = jnp.maximum(jnp.maximum(parts[0], parts[1]), jnp.maximum(parts[2], parts[3]))
                high = jnp.max(high, axis=1, keepdims=True) * log_scale
                if opening:
                    new = high
                else:
                    old = top[a, rows][:, :1]
                    new = jnp.maximum(old, high)
                e = jnp.exp2(s * log_scale - new)
                total = (e[:, 0:128] + e[:, 128:256]) + (e[:, 256:384] + e[:, 384:512])
                weighted = dot(e.astype(BF), v)
                if opening:
                    tot[a, rows] = total
                    acc[a, rows] = weighted
                else:
                    fade = jnp.exp2(old - new)
                    tot[a, rows] = tot[a, rows] * fade + total
                    acc[a, rows] = acc[a, rows] * fade + weighted
                top[a, rows] = jnp.broadcast_to(new, (256, 128))

    attend(place, u, True, True)

    ksteps = keys.steps()
    csteps = columns.steps()

    @pl.loop(0, 15)
    def _(t):
        for k in range(15):
            on_step(t, k, csteps[k][0] + ksteps[k][0])
        at_z = lax.rem(z + pick(t, dzs[1:]) + 4, 4)
        at_u = lax.rem(u + pick(t, dus[1:]) + 4, 4)
        index = at_z * 4 + at_u
        before = jnp.logical_and(at_z == z, jnp.logical_and(core == 0, at_u < u))

        @pl.when(jnp.logical_or(at_z < z, before))
        def _():
            attend(index, at_u, False, False)

        @pl.when(jnp.logical_and(at_z == z, core == 1))
        def _():
            attend(index, at_u, True, False)

    links.arrived(lrecv, xss.at[0], xrs.at[0])
    o1 = acc[0] / jnp.sum(tot[0], axis=1, keepdims=True)
    o2 = acc[1] / jnp.sum(tot[1], axis=1, keepdims=True)
    mixed = o1 - lrecv[0:1, 0:1] * o2
    norm = lax.rsqrt(jnp.mean(mixed * mixed, axis=1, keepdims=True) + EPS_NORM)
    mine[...] = (mixed * norm * gain[...]).astype(BF)

    def partial(dw):
        start = NEAR.index(dw) * 128
        return dot(mine[start : start + 128, :], obuf[...])

    term = partial(2)
    fsend[0] = term[:64].astype(BF)
    plain(fsend.at[0], frecv.at[0], xss.at[1], xrs.at[1], "w", 1)
    fsend[1] = term[64:].astype(BF)
    plain(fsend.at[1], frecv.at[1], xss.at[2], xrs.at[2], "w", -1)
    term = partial(1)
    nsend[1, 1] = term[64:].astype(BF)
    plain(nsend.at[1, 1], nrecv.at[1, 1], xss.at[3], xrs.at[3], "w", 1)
    keep[0] = term[:64]
    term = partial(-1)
    nsend[0, 0] = term[:64].astype(BF)
    plain(nsend.at[0, 0], nrecv.at[0, 0], xss.at[4], xrs.at[4], "w", -1)
    keep[1] = term[64:]
    term = partial(0)
    sums[0] = term[:64]
    sums[1] = term[64:]
    links.arrived(frecv.at[0], xss.at[1], xrs.at[1])
    nsend[1, 0] = (keep[0] + frecv[0].astype(F32)).astype(BF)
    plain(nsend.at[1, 0], nrecv.at[1, 0], xss.at[5], xrs.at[5], "w", 1)
    links.arrived(frecv.at[1], xss.at[2], xrs.at[2])
    nsend[0, 1] = (keep[1] + frecv[1].astype(F32)).astype(BF)
    plain(nsend.at[0, 1], nrecv.at[0, 1], xss.at[6], xrs.at[6], "w", -1)
    links.arrived(nrecv.at[1, 1], xss.at[3], xrs.at[3])
    sums[1] += nrecv[1, 1].astype(F32)
    links.arrived(nrecv.at[0, 0], xss.at[4], xrs.at[4])
    sums[0] += nrecv[0, 0].astype(F32)
    links.arrived(nrecv.at[1, 0], xss.at[5], xrs.at[5])
    sums[0] += nrecv[1, 0].astype(F32)
    links.arrived(nrecv.at[0, 1], xss.at[6], xrs.at[6])
    sums[1] += nrecv[0, 1].astype(F32)
    osend[...] = sums[1 - core].astype(BF)
    plain(osend, orecv, xss.at[7], xrs.at[7], "core")
    links.arrived(orecv, xss.at[7], xrs.at[7])
    out[...] = (sums[core] + orecv[...].astype(F32)).astype(BF)
    links.drain()


def on_device(tokens, query_one, query_two, key_one, key_two, value_weight, out_weight, lambdas, head_gain):
    inverse = 1.0 / np.float32(ROPE_BASE) ** (np.arange(0, QK, 2, dtype=np.float32) / np.float32(QK))
    vm = pl.BlockSpec(memory_space=pltpu.VMEM)
    dma = pltpu.SemaphoreType.DMA
    return pl.pallas_call(
        layer_kernel,
        out_shape=jax.ShapeDtypeStruct((64, 4096), BF),
        in_specs=[vm] * 7 + [pl.BlockSpec(memory_space=pltpu.SMEM)] + [vm] * 2,
        out_specs=vm,
        scratch_shapes=[
            pltpu.VMEM((ROWS, QK), F32),
            pltpu.VMEM((ROWS, QK), F32),
            pltpu.VMEM((ROWS, 4096), BF),
            pltpu.VMEM((4096, 768), BF),
            pltpu.VMEM((ROWS, 768), F32),
            pltpu.VMEM((2, ROWS, QK), BF),
            pltpu.VMEM((8192, 512), BF),
            pltpu.VMEM((256, 4096), BF),
            pltpu.VMEM((2, ROWS, V), F32),
            pltpu.VMEM((2, ROWS, 128), F32),
            pltpu.VMEM((2, ROWS, 128), F32),
            pltpu.VMEM((2, 64, 4096), BF),
            pltpu.VMEM((2, 64, 4096), BF),
            pltpu.VMEM((2, 2, 64, 4096), BF),
            pltpu.VMEM((2, 2, 64, 4096), BF),
            pltpu.VMEM((2, 64, 4096), F32),
            pltpu.VMEM((2, 64, 4096), F32),
            pltpu.VMEM((64, 4096), BF),
            pltpu.VMEM((64, 4096), BF),
            pltpu.VMEM((ROWS, V), BF),
            pltpu.VMEM((8, 128), F32),
            pltpu.VMEM((8, 128), F32),
            dma((1,)),
            dma((40,)), dma((40,)),
            dma((40,)), dma((40,)),
            dma((40,)), dma((40,)),
            dma((7,)), dma((7,)),
            dma((12,)), dma((12,)),
            dma((8,)), dma((8,)),
        ],
        compiler_params=pltpu.CompilerParams(
            collective_id=0, has_side_effects=True, vmem_limit_bytes=62 * 1024 * 1024
        ),
    )(tokens, query_one, query_two, key_one, key_two, value_weight, out_weight, lambdas, head_gain[None], jnp.asarray(inverse[None], F32))


def solution(mesh):
    fine = Mesh(mesh.devices.reshape(4, 4, 2, 4), AXES)
    sp = ("z", "y", "core")
    in_specs = (
        P((*sp, "x"), None),
        P(sp, "x"),
        P(sp, "x"),
        P(sp, "x"),
        P(sp, "x"),
        P(sp, "x"),
        P("x", sp),
        P("x"),
        P(),
    )
    return jax.shard_map(on_device, mesh=fine, in_specs=in_specs, out_specs=P((*sp, "x"), None), check_vma=False)
```

time: 135 us -> 122 us (0.904); the launches traced: 132 us -> 122 us
  Pallas kernels: 130 us -> 120 us
    pallas_call x1, Pallas kernels: 130 us -> 120 us  [on_device(): pl.pallas_call(layer_kernel, out_shape=jax.ShapeDtypeStruct((64, 4096), B...]
where the time goes in v1:
time: 122 us
  Pallas kernels  120 us (98%)
  local copies, waits for them, and re-layouts  1.87 us (2%)
    pallas_call x1, Pallas kernels, on_device(): pl.pallas_call(layer_kernel, out_shape=jax.ShapeDtypeStruct((64, 4096), B...  120 us

profile of v1, /device:TPU:1, one launch (start us, length us, event | category | flops | bytes accessed | tf_op | source)
XLA Modules:
  0.0 121.5 jit_solution(13829152408388476949)
XLA Ops:
  0.0 119.6 %shard_map.100 = bf16[64,4096]{1,0:T(8,128)(2,1)} custom-call(bf16[64,4096]{1,0:T(8,128)(2,1)} %tok.1, bf16[128,256]{1,0:T(8,128)(2,1)} %wq1.1, bf16[128,256]{1,0:T(8,128)(2,1)} %wq2.1, bf16[128,256]{1,0:T(8,128)(2,1)} %wk1.1, bf16[128,256]{1,0:T(8,128)(2,1)} %wk2.1, bf16[128,512]{1,0:T(8,128)(2,1)} %wv.1, bf16[512,128]{1,0:T(8,128)(2,1)} %wo.1, f32[2]{0:T(128)} %lam.1, ...), custom_call_target="tpu_custom_call" | custom-call | tf_op jit(solution)/shard_map/pallas_call | solution.py:453
  119.6 1.9 %copy.12 = bf16[64,4096]{1,0:T(8,128)(2,1)} copy(bf16[64,4096]{1,0:T(8,128)(2,1)} %shard_map.100) | data formatting | bytes 1048576

commit v2 on v1

--- a/solution.py
+++ b/solution.py
@@ -29,6 +29,7 @@
         self.u = self.y * (1 - self.core) + self.x * self.core
         self.w = self.x * (1 - self.core) + self.y * self.core
         self.sent = []
+        self.later = []
 
     def peer(self, axis, step):
         if axis == "core":
@@ -36,13 +37,13 @@
         if axis == "even":
             return {"core": 0}
         if axis == "odd":
-            return {"y": self.x, "core": 1, "x": self.y}
+            return {"y": self.x, "core": 1, "x": lax.rem(2 * self.x - self.y + 4, 4)}
         if axis == "z":
             return {"z": lax.rem(self.z + (step + 4), 4)}
         along = self.core if axis == "u" else 1 - self.core
         return {"y": lax.rem(self.y + (4 + step * (1 - along)), 4), "x": lax.rem(self.x + (4 + step * along), 4)}
 
-    def send(self, views, axis, step, only=None):
+    def send(self, views, axis, step, only=None, noted=True):
         def copy():
             return pltpu.make_async_remote_copy(*views(), device_id=self.peer(axis, step), device_id_type=MESH)
 
@@ -50,7 +51,8 @@
             copy().start()
         else:
             pl.when(only)(lambda: copy().start())
-        self.sent.append((copy, only))
+        if noted:
+            self.sent.append((copy, only))
 
     def arrived(self, view, ssem, rsem):
         pltpu.make_async_remote_copy(view, view, ssem, rsem, device_id=self.peer("core", 1), device_id_type=MESH).wait_recv()
@@ -61,11 +63,14 @@
                 copy().wait_send()
             else:
                 pl.when(only)(lambda copy=copy: copy().wait_send())
+        for view, ssem in self.later:
+            pltpu.make_async_remote_copy(view, view, ssem, ssem, device_id=self.peer("core", 1), device_id_type=MESH).wait_send()
 
 
 class TorusGather:
-    def __init__(self, links, piece, ssem, rsem):
+    def __init__(self, links, piece, ssem, rsem, all_sent):
         self.links, self.piece, self.ssem, self.rsem = links, piece, ssem, rsem
+        links.later.append((all_sent, ssem.at[0]))
 
     def ref(self, part, dp, ds, sub=None):
         dz, du = (ds, dp) if part == 0 else (dp, ds)
@@ -79,13 +84,13 @@
 
         def views():
             view = self.ref(part, dp, ds, sub)
-            return view, view, self.ssem.at[k], self.rsem.at[k]
-
-        self.links.send(views, self.axis(part, second), step)
+            return view, view, self.ssem.at[0], self.rsem.at[k]
+
+        self.links.send(views, self.axis(part, second), step, noted=False)
 
     def wait(self, part, key, dp, ds, sub):
         k = part * 20 + key
-        self.links.arrived(self.ref(part, dp, ds, sub), self.ssem.at[k], self.rsem.at[k])
+        self.links.arrived(self.ref(part, dp, ds, sub), self.ssem.at[0], self.rsem.at[k])
 
     def spread(self, part, dp):
         i = NEAR.index(dp)
@@ -180,12 +185,21 @@
 ):
     links = Links()
     z, y, core, x, u, w = links.z, links.y, links.core, links.x, links.u, links.w
+    other = 1 - core
     chip = z * 4 + y
     place = z * 4 + u
     log_scale = QK ** (-0.5) * LOG2E
 
     def slot(dz, du):
         return lax.rem(z + (dz + 4), 4) * 4 + lax.rem(u + (du + 4), 4)
+
+    def depth_of(at_z, at_u):
+        return at_z * 4 + jnp.where(core == 0, at_u, lax.rem(2 * w - at_u + 4, 4))
+
+    def near_depth(dz, du):
+        return depth_of(lax.rem(z + (dz + 4), 4), lax.rem(u + (du + 4), 4))
+
+    own_depth = depth_of(z, u)
 
     def plain(src, dst, ssem, rsem, axis, step=1, only=None):
         links.send(lambda: (src, dst, ssem, rsem), axis, step, only)
@@ -197,8 +211,9 @@
 
     @pl.when(jnp.logical_and(core == 1, crossed))
     def _():
-        for other in (0, 1):
-            pl.semaphore_signal(barrier, inc=1, device_id={"y": x, "core": other, "x": y}, device_id_type=MESH)
+        for c in (0, 1):
+            source = {"y": lax.rem(2 * y - x + 4, 4), "core": c, "x": y}
+            pl.semaphore_signal(barrier, inc=1, device_id=source, device_id_type=MESH)
 
     pl.semaphore_wait(barrier, 7 + jnp.where(crossed, 1, 0))
 
@@ -231,29 +246,29 @@
     hand_over(range(5))
     plain(tok, tbuf.at[window(core * 64, 64), :], tss.at[6], trs.at[6], "core")
     plain(tok, tbuf.at[window(NEAR.index(-1) * 128 + core * 64, 64), :], tss.at[core], trs.at[core], "w", 1)
-    plain(tok, tbuf.at[window(NEAR.index(1) * 128 + core * 64, 64), :], tss.at[2 + core], trs.at[2 + core], "w", -1)
     hand_over([5])
 
     for c in (0, 1):
         column = 0
         for i, width in enumerate((QK, QK, QK, QK, V)):
-            view = wbuf.at[window(place * 256 + c * 128, 128), pl.ds(column, width)]
+            view = wbuf.at[window(own_depth * 256 + c * 128, 128), pl.ds(column, width)]
             links.arrived(view, sss.at[i], srs.at[c * 6 + i])
             column += width
 
     def wpiece(dz, du, part, sub):
-        start = slot(dz, du) * 256 + part * 128
+        start = near_depth(dz, du) * 256 + part * 128
         if sub is None:
             return wbuf.at[window(start, 128), :]
         return wbuf.at[window(start + sub * 64, 64), :]
 
-    weights = TorusGather(links, wpiece, wss, wrs)
+    weights = TorusGather(links, wpiece, wss, wrs, wbuf.at[pl.ds(0, 3840), :])
     weights.begin()
 
-    links.arrived(trows(0, 1 - core), tss.at[6], trs.at[6])
-    sibling = trows(0, 1 - core)
-    plain(sibling, tbuf.at[window(NEAR.index(-1) * 128 + (1 - core) * 64, 64), :], tss.at[1 - core], trs.at[1 - core], "w", 1)
-    plain(sibling, tbuf.at[window(NEAR.index(1) * 128 + (1 - core) * 64, 64), :], tss.at[3 - core], trs.at[3 - core], "w", -1)
+    links.arrived(trows(0, other), tss.at[6], trs.at[6])
+    sibling = trows(0, other)
+    plain(sibling, tbuf.at[window(NEAR.index(1) * 128 + other * 64, 64), :], tss.at[2 + other], trs.at[2 + other], "w", -1)
+    plain(tok, tbuf.at[window(NEAR.index(1) * 128 + core * 64, 64), :], tss.at[2 + core], trs.at[2 + core], "w", -1)
+    plain(sibling, tbuf.at[window(NEAR.index(-1) * 128 + other * 64, 64), :], tss.at[other], trs.at[other], "w", 1)
 
     lown[...] = jnp.full((8, 128), jnp.where(core == 0, lam[0], lam[1]), F32)
 
@@ -261,17 +276,19 @@
         links.send(lambda: (trows(dw, c), trows(2, c), tss.at[k], trs.at[k]), "w", step)
 
     def near_tokens():
-        for c in (0, 1):
-            links.arrived(trows(-1, c), tss.at[c], trs.at[c])
-        pass_on(-1, 0, 4, 1)
-        for c in (0, 1):
-            links.arrived(trows(1, c), tss.at[2 + c], trs.at[2 + c])
-        pass_on(1, 1, 5, -1)
+        links.arrived(trows(-1, core), tss.at[core], trs.at[core])
+        pass_on(-1, core, 4, 1)
+        links.arrived(trows(1, other), tss.at[2 + other], trs.at[2 + other])
+        pass_on(1, other, 5, -1)
+
+    def near_tokens_rest():
+        links.arrived(trows(-1, other), tss.at[other], trs.at[other])
+        links.arrived(trows(1, core), tss.at[2 + core], trs.at[2 + core])
         own_tokens.wait()
 
     def far_tokens():
-        for c in (0, 1):
-            links.arrived(trows(2, c), tss.at[4 + c], trs.at[4 + c])
+        links.arrived(trows(2, core), tss.at[4], trs.at[4])
+        links.arrived(trows(2, other), tss.at[5], trs.at[5])
 
     def positions(ids, at_u):
         rel = ids // 128
@@ -290,7 +307,8 @@
     proj[...] = jnp.zeros_like(proj)
 
     steps = weights.steps()
-    early = [action for actions, _ in steps[:8] for action in actions] + [near_tokens]
+    early = [action for actions, _ in steps[:6] for action in actions] + [near_tokens]
+    early += [action for actions, _ in steps[6:8] for action in actions] + [near_tokens_rest]
     dzs = [0] + [d for _, (d, _) in steps]
     dus = [0] + [d for _, (_, d) in steps]
 
@@ -301,19 +319,19 @@
         on_step(t, 11, [lambda: weights.third(-1)])
         on_step(t, 13, [lambda: weights.third(1)])
         on_step(t, 15, [lambda: weights.third(2)])
-        depth = window(slot(pick(t, dzs), pick(t, dus)) * 256, 256)
+        depth = window(near_depth(pick(t, dzs), pick(t, dus)) * 256, 256)
         proj[0:384, :] += dot(tbuf[0:384, depth], wbuf[depth, :])
 
     def opiece(dz, du, part, sub):
-        cols = window(slot(dz, du) * 256, 256)
+        cols = window(near_depth(dz, du) * 256, 256)
         start, size = ((0, 64), (64, 192))[part]
         if sub is None:
             return obuf.at[pl.ds(start, size), cols]
         return obuf.at[pl.ds(start + sub * (size // 2), size // 2), cols]
 
     for c in (0, 1):
-        links.arrived(obuf.at[:, window((place * 2 + c) * 128, 128)], sss.at[5], srs.at[c * 6 + 5])
-    columns = TorusGather(links, opiece, oss, ors)
+        links.arrived(obuf.at[:, window((own_depth * 2 + c) * 128, 128)], sss.at[5], srs.at[c * 6 + 5])
+    columns = TorusGather(links, opiece, oss, ors, obuf.at[:, pl.ds(0, 3840)])
     columns.begin()
     far_tokens()
     proj[384:512, :] = dot(tbuf[384:512, :], wbuf[...])
@@ -335,7 +353,7 @@
             return kvbuf.at[pl.ds(pl.multiple_of(base, 128), size), :]
         return kvbuf.at[pl.ds(pl.multiple_of(base + sub * (size // 2), 64), size // 2), :]
 
-    keys = TorusGather(links, kpiece, kss, krs)
+    keys = TorusGather(links, kpiece, kss, krs, kvbuf.at[pl.ds(0, 7680), :])
     keys.begin()
     crosses = jnp.logical_and(core == 1, crossed)
     plain(lown, lrecv, xss.at[0], xrs.at[0], "odd", only=crosses)
@@ -439,7 +457,7 @@
     sums[0] += nrecv[1, 0].astype(F32)
     links.arrived(nrecv.at[0, 1], xss.at[6], xrs.at[6])
     sums[1] += nrecv[0, 1].astype(F32)
-    osend[...] = sums[1 - core].astype(BF)
+    osend[...] = sums[other].astype(BF)
     plain(osend, orecv, xss.at[7], xrs.at[7], "core")
     links.arrived(orecv, xss.at[7], xrs.at[7])
     out[...] = (sums[core] + orecv[...].astype(F32)).astype(BF)
@@ -479,9 +497,9 @@
             pltpu.VMEM((8, 128), F32),
             pltpu.VMEM((8, 128), F32),
             dma((1,)),
-            dma((40,)), dma((40,)),
-            dma((40,)), dma((40,)),
-            dma((40,)), dma((40,)),
+            dma((1,)), dma((40,)),
+            dma((1,)), dma((40,)),
+            dma((1,)), dma((40,)),
             dma((7,)), dma((7,)),
             dma((12,)), dma((12,)),
             dma((8,)), dma((8,)),

time: 122 us -> 117 us (0.959)
  Pallas kernels: 120 us -> 115 us
    pallas_call x1, Pallas kernels: 120 us -> 115 us  [on_device(): pl.pallas_call(layer_kernel, out_shape=jax.ShapeDtypeStruct((64, 4096), B...]
where the time goes in v2:
time: 117 us
  Pallas kernels  115 us (98%)
  local copies, waits for them, and re-layouts  1.87 us (2%)
    pallas_call x1, Pallas kernels, on_device(): pl.pallas_call(layer_kernel, out_shape=jax.ShapeDtypeStruct((64, 4096), B...  115 us

profile of v2, /device:TPU:1, one launch (start us, length us, event | category | flops | bytes accessed | tf_op | source)
XLA Modules:
  0.0 117.2 jit_solution(16523024952069382996)
XLA Ops:
  0.0 115.3 %shard_map.100 = bf16[64,4096]{1,0:T(8,128)(2,1)} custom-call(bf16[64,4096]{1,0:T(8,128)(2,1)} %tok.1, bf16[128,256]{1,0:T(8,128)(2,1)} %wq1.1, bf16[128,256]{1,0:T(8,128)(2,1)} %wq2.1, bf16[128,256]{1,0:T(8,128)(2,1)} %wk1.1, bf16[128,256]{1,0:T(8,128)(2,1)} %wk2.1, bf16[128,512]{1,0:T(8,128)(2,1)} %wv.1, bf16[512,128]{1,0:T(8,128)(2,1)} %wo.1, f32[2]{0:T(128)} %lam.1, ...), custom_call_target="tpu_custom_call" | custom-call | tf_op jit(solution)/shard_map/pallas_call | solution.py:471
  115.3 1.9 %copy.12 = bf16[64,4096]{1,0:T(8,128)(2,1)} copy(bf16[64,4096]{1,0:T(8,128)(2,1)} %shard_map.100) | data formatting | bytes 1048576

commit v3 on v2

--- a/solution.py
+++ b/solution.py
@@ -36,6 +36,8 @@
             return {"core": 1 - self.core}
         if axis == "even":
             return {"core": 0}
+        if axis == "turned":
+            return {"y": self.x, "core": 0, "x": self.y}
         if axis == "odd":
             return {"y": self.x, "core": 1, "x": lax.rem(2 * self.x - self.y + 4, 4)}
         if axis == "z":
@@ -180,7 +182,7 @@
 def layer_kernel(
     tok, wq1, wq2, wk1, wk2, wv, wo, lam, gain, inverse, out, cos, sin,
     tbuf, wbuf, proj, qbuf, kvbuf, obuf, acc, top, tot,
-    fsend, frecv, nsend, nrecv, keep, sums, osend, orecv, mine, lown, lrecv,
+    abuf, osum, fsend, passing, nsend, fin, sib, lown, lrecv,
     lsem, wss, wrs, kss, krs, oss, ors, tss, trs, sss, srs, xss, xrs,
 ):
     links = Links()
@@ -215,7 +217,12 @@
             source = {"y": lax.rem(2 * y - x + 4, 4), "core": c, "x": y}
             pl.semaphore_signal(barrier, inc=1, device_id=source, device_id_type=MESH)
 
-    pl.semaphore_wait(barrier, 7 + jnp.where(crossed, 1, 0))
+    @pl.when(jnp.logical_and(core == 0, crossed))
+    def _():
+        for c in (0, 1):
+            pl.semaphore_signal(barrier, inc=1, device_id={"y": x, "core": c, "x": y}, device_id_type=MESH)
+
+    pl.semaphore_wait(barrier, 7 + jnp.where(crossed, 2, 0))
 
     def trows(dw, c):
         return tbuf.at[window(NEAR.index(dw) * 128 + c * 64, 64), :]
@@ -230,7 +237,6 @@
         cols = pl.ds(column, width)
         items.append((ref.at[:, pl.ds(0, width)], ref.at[:, pl.ds(width, width)], wbuf.at[own_rows, cols]))
         column += width
-    items.append((wo.at[pl.ds(0, 256), :], wo.at[pl.ds(256, 256), :], obuf.at[:, window((chip * 2 + core) * 128, 128)]))
     stays = jnp.logical_and(core == 1, x == y)
     leaves = jnp.logical_not(stays)
 
@@ -243,10 +249,20 @@
             plain(even, dst, sss.at[i], srs.at[k], "even", only=core == 1)
             pl.when(core == 0)(lambda: pltpu.make_async_copy(even, dst, srs.at[k]).start())
 
+    def hand_over_out():
+        dst = obuf.at[window(x * 256, 256), window(z * 256 + core * 128, 128)]
+        even, odd = wo.at[pl.ds(0, 256), :], wo.at[pl.ds(256, 256), :]
+        k = core * 6 + 5
+        here = jnp.logical_and(core == 0, x == y)
+        plain(even, dst, sss.at[5], srs.at[k], "turned", only=jnp.logical_not(here))
+        pl.when(here)(lambda: pltpu.make_async_copy(even, dst, srs.at[k]).start())
+        plain(odd, dst, sss.at[11], srs.at[k], "core", only=core == 0)
+        pl.when(core == 1)(lambda: pltpu.make_async_copy(odd, dst, srs.at[k]).start())
+
     hand_over(range(5))
     plain(tok, tbuf.at[window(core * 64, 64), :], tss.at[6], trs.at[6], "core")
     plain(tok, tbuf.at[window(NEAR.index(-1) * 128 + core * 64, 64), :], tss.at[core], trs.at[core], "w", 1)
-    hand_over([5])
+    hand_over_out()
 
     for c in (0, 1):
         column = 0
@@ -323,15 +339,16 @@
         proj[0:384, :] += dot(tbuf[0:384, depth], wbuf[depth, :])
 
     def opiece(dz, du, part, sub):
-        cols = window(near_depth(dz, du) * 256, 256)
+        cols = window(lax.rem(z + (dz + 4), 4) * 256, 256)
         start, size = ((0, 64), (64, 192))[part]
+        base = lax.rem(u + (du + 4), 4) * 256 + start
         if sub is None:
-            return obuf.at[pl.ds(start, size), cols]
-        return obuf.at[pl.ds(start + sub * (size // 2), size // 2), cols]
+            return obuf.at[pl.ds(pl.multiple_of(base, 64), size), cols]
+        return obuf.at[pl.ds(pl.multiple_of(base + sub * (size // 2), 32), size // 2), cols]
 
     for c in (0, 1):
-        links.arrived(obuf.at[:, window((own_depth * 2 + c) * 128, 128)], sss.at[5], srs.at[c * 6 + 5])
-    columns = TorusGather(links, opiece, oss, ors, obuf.at[:, pl.ds(0, 3840)])
+        links.arrived(obuf.at[window(u * 256, 256), window(z * 256 + c * 128, 128)], sss.at[5], srs.at[c * 6 + 5])
+    columns = TorusGather(links, opiece, oss, ors, obuf.at[pl.ds(0, 960), :])
     columns.begin()
     far_tokens()
     proj[384:512, :] = dot(tbuf[384:512, :], wbuf[...])
@@ -398,11 +415,14 @@
 
     ksteps = keys.steps()
     csteps = columns.steps()
+    early_columns = [[] for _ in range(15)]
+    for k in range(15):
+        early_columns[max(k - 1, 0)] += csteps[k][0]
 
     @pl.loop(0, 15)
     def _(t):
         for k in range(15):
-            on_step(t, k, csteps[k][0] + ksteps[k][0])
+            on_step(t, k, early_columns[k] + ksteps[k][0])
         at_z = lax.rem(z + pick(t, dzs[1:]) + 4, 4)
         at_u = lax.rem(u + pick(t, dus[1:]) + 4, 4)
         index = at_z * 4 + at_u
@@ -417,50 +437,94 @@
             attend(index, at_u, True, False)
 
     links.arrived(lrecv, xss.at[0], xrs.at[0])
-    o1 = acc[0] / jnp.sum(tot[0], axis=1, keepdims=True)
-    o2 = acc[1] / jnp.sum(tot[1], axis=1, keepdims=True)
-    mixed = o1 - lrecv[0:1, 0:1] * o2
-    norm = lax.rsqrt(jnp.mean(mixed * mixed, axis=1, keepdims=True) + EPS_NORM)
-    mine[...] = (mixed * norm * gain[...]).astype(BF)
-
-    def partial(dw):
-        start = NEAR.index(dw) * 128
-        return dot(mine[start : start + 128, :], obuf[...])
-
-    term = partial(2)
-    fsend[0] = term[:64].astype(BF)
-    plain(fsend.at[0], frecv.at[0], xss.at[1], xrs.at[1], "w", 1)
-    fsend[1] = term[64:].astype(BF)
-    plain(fsend.at[1], frecv.at[1], xss.at[2], xrs.at[2], "w", -1)
-    term = partial(1)
-    nsend[1, 1] = term[64:].astype(BF)
-    plain(nsend.at[1, 1], nrecv.at[1, 1], xss.at[3], xrs.at[3], "w", 1)
-    keep[0] = term[:64]
-    term = partial(-1)
-    nsend[0, 0] = term[:64].astype(BF)
-    plain(nsend.at[0, 0], nrecv.at[0, 0], xss.at[4], xrs.at[4], "w", -1)
-    keep[1] = term[64:]
-    term = partial(0)
-    sums[0] = term[:64]
-    sums[1] = term[64:]
-    links.arrived(frecv.at[0], xss.at[1], xrs.at[1])
-    nsend[1, 0] = (keep[0] + frecv[0].astype(F32)).astype(BF)
-    plain(nsend.at[1, 0], nrecv.at[1, 0], xss.at[5], xrs.at[5], "w", 1)
-    links.arrived(frecv.at[1], xss.at[2], xrs.at[2])
-    nsend[0, 1] = (keep[1] + frecv[1].astype(F32)).astype(BF)
-    plain(nsend.at[0, 1], nrecv.at[0, 1], xss.at[6], xrs.at[6], "w", -1)
-    links.arrived(nrecv.at[1, 1], xss.at[3], xrs.at[3])
-    sums[1] += nrecv[1, 1].astype(F32)
-    links.arrived(nrecv.at[0, 0], xss.at[4], xrs.at[4])
-    sums[0] += nrecv[0, 0].astype(F32)
-    links.arrived(nrecv.at[1, 0], xss.at[5], xrs.at[5])
-    sums[0] += nrecv[1, 0].astype(F32)
-    links.arrived(nrecv.at[0, 1], xss.at[6], xrs.at[6])
-    sums[1] += nrecv[0, 1].astype(F32)
-    osend[...] = sums[other].astype(BF)
-    plain(osend, orecv, xss.at[7], xrs.at[7], "core")
-    links.arrived(orecv, xss.at[7], xrs.at[7])
-    out[...] = (sums[core] + orecv[...].astype(F32)).astype(BF)
+
+    def finish(h):
+        rows = pl.ds(h * 256, 256)
+        o1 = acc[0, rows] / jnp.sum(tot[0, rows], axis=1, keepdims=True)
+        o2 = acc[1, rows] / jnp.sum(tot[1, rows], axis=1, keepdims=True)
+        mixed = o1 - lrecv[0:1, 0:1] * o2
+        norm = lax.rsqrt(jnp.mean(mixed * mixed, axis=1, keepdims=True) + EPS_NORM)
+        abuf[0, rows] = (mixed * norm * gain[...]).astype(BF)
+
+    def heads(k, h):
+        return abuf.at[k, pl.ds(h * 256, 256), :]
+
+    def along(src, dst, k, step):
+        plain(src, dst, xss.at[k], xrs.at[k], "w", step)
+
+    def got(view, k):
+        links.arrived(view, xss.at[k], xrs.at[k])
+
+    seen = set()
+
+    def add(dw, h):
+        head = window(lax.rem(w + (dw + 4), 4) * 256, 256)
+        term = dot(abuf[NEAR.index(dw), h * 256 : (h + 1) * 256, :], obuf[head, :])
+        for b in (0, 1):
+            target = (dw + NEAR[2 * h + b]) % 4
+            j = NEAR.index(-1 if target == 3 else target)
+            block = term[b * 128 : (b + 1) * 128]
+            if j in seen:
+                osum[j] += block
+            else:
+                osum[j] = block
+            seen.add(j)
+
+    finish(0)
+    along(heads(0, 0), heads(1, 0), 1, 1)
+    finish(1)
+    along(heads(0, 1), heads(2, 1), 4, -1)
+    along(heads(0, 0), heads(2, 0), 3, -1)
+    along(heads(0, 1), heads(1, 1), 2, 1)
+    add(0, 0)
+    add(0, 1)
+    got(heads(1, 0), 1)
+    along(heads(1, 0), heads(3, 0), 5, 1)
+    got(heads(2, 1), 4)
+    along(heads(2, 1), heads(3, 1), 6, -1)
+    add(-1, 0)
+    add(1, 1)
+    got(heads(1, 1), 2)
+    add(-1, 1)
+    got(heads(2, 0), 3)
+    add(1, 0)
+    got(heads(3, 0), 5)
+    add(2, 0)
+    got(heads(3, 1), 6)
+    add(2, 1)
+
+    for r, step in ((0, 1), (1, -1)):
+        fsend[r] = osum[3, r * 64 : (r + 1) * 64].astype(BF)
+        along(fsend.at[r], passing.at[r], 7 + r, step)
+    nsend[0] = osum[2].astype(BF)
+    along(nsend.at[0], fin.at[1], 9, 1)
+    nsend[1] = osum[1].astype(BF)
+    along(nsend.at[1], fin.at[2], 10, -1)
+    fin[0] = osum[0].astype(BF)
+    other_rows = window(other * 64, 64)
+
+    def to_sibling(k):
+        at_w = lax.rem(w + (NEAR[k] + 4), 4)
+        plain(fin.at[k, other_rows, :], sib.at[at_w], xss.at[13 + k], xrs.at[13 + at_w], "core")
+
+    to_sibling(0)
+    for r, step in ((0, 1), (1, -1)):
+        got(passing.at[r], 7 + r)
+        along(passing.at[r], fin.at[3, pl.ds(r * 64, 64), :], 11 + r, step)
+    got(fin.at[1], 9)
+    to_sibling(1)
+    got(fin.at[2], 10)
+    to_sibling(2)
+    got(fin.at[3, pl.ds(0, 64), :], 11)
+    got(fin.at[3, pl.ds(64, 64), :], 12)
+    to_sibling(3)
+    own_part = window(core * 64, 64)
+    for k in range(4):
+        at_w = lax.rem(w + (NEAR[k] + 4), 4)
+        links.arrived(sib.at[at_w], xss.at[13 + k], xrs.at[13 + at_w])
+        both = (fin[k, own_part, :].astype(F32) + sib[at_w].astype(F32)).astype(BF)
+        for c in range(4):
+            out[:, window((c * 4 + at_w) * 256, 256)] = both[:, c * 256 : (c + 1) * 256]
     links.drain()
 
 
@@ -481,19 +545,17 @@
             pltpu.VMEM((ROWS, 768), F32),
             pltpu.VMEM((2, ROWS, QK), BF),
             pltpu.VMEM((8192, 512), BF),
-            pltpu.VMEM((256, 4096), BF),
+            pltpu.VMEM((1024, 1024), BF),
             pltpu.VMEM((2, ROWS, V), F32),
             pltpu.VMEM((2, ROWS, 128), F32),
             pltpu.VMEM((2, ROWS, 128), F32),
-            pltpu.VMEM((2, 64, 4096), BF),
-            pltpu.VMEM((2, 64, 4096), BF),
-            pltpu.VMEM((2, 2, 64, 4096), BF),
-            pltpu.VMEM((2, 2, 64, 4096), BF),
-            pltpu.VMEM((2, 64, 4096), F32),
-            pltpu.VMEM((2, 64, 4096), F32),
-            pltpu.VMEM((64, 4096), BF),
-            pltpu.VMEM((64, 4096), BF),
-            pltpu.VMEM((ROWS, V), BF),
+            pltpu.VMEM((4, ROWS, V), BF),
+            pltpu.VMEM((4, 128, 1024), F32),
+            pltpu.VMEM((2, 64, 1024), BF),
+            pltpu.VMEM((2, 64, 1024), BF),
+            pltpu.VMEM((2, 128, 1024), BF),
+            pltpu.VMEM((4, 128, 1024), BF),
+            pltpu.VMEM((4, 64, 1024), BF),
             pltpu.VMEM((8, 128), F32),
             pltpu.VMEM((8, 128), F32),
             dma((1,)),
@@ -502,7 +564,7 @@
             dma((1,)), dma((40,)),
             dma((7,)), dma((7,)),
             dma((12,)), dma((12,)),
-            dma((8,)), dma((8,)),
+            dma((17,)), dma((17,)),
         ],
         compiler_params=pltpu.CompilerParams(
             collective_id=0, has_side_effects=True, vmem_limit_bytes=62 * 1024 * 1024

time: 117 us -> 115 us (0.983)
  Pallas kernels: 115 us -> 113 us
    pallas_call x1, Pallas kernels: 115 us -> 113 us  [on_device(): pl.pallas_call(layer_kernel, out_shape=jax.ShapeDtypeStruct((64, 4096), B...]
where the time goes in v3:
time: 115 us
  Pallas kernels  113 us (98%)
  local copies, waits for them, and re-layouts  1.87 us (2%)
    pallas_call x1, Pallas kernels, on_device(): pl.pallas_call(layer_kernel, out_shape=jax.ShapeDtypeStruct((64, 4096), B...  113 us

profile of v3, /device:TPU:1, one launch (start us, length us, event | category | flops | bytes accessed | tf_op | source)
XLA Modules:
  0.0 115.0 jit_solution(1237962713680210188)
XLA Ops:
  0.0 113.1 %shard_map.100 = bf16[64,4096]{1,0:T(8,128)(2,1)} custom-call(bf16[64,4096]{1,0:T(8,128)(2,1)} %tok.1, bf16[128,256]{1,0:T(8,128)(2,1)} %wq1.1, bf16[128,256]{1,0:T(8,128)(2,1)} %wq2.1, bf16[128,256]{1,0:T(8,128)(2,1)} %wk1.1, bf16[128,256]{1,0:T(8,128)(2,1)} %wk2.1, bf16[128,512]{1,0:T(8,128)(2,1)} %wv.1, bf16[512,128]{1,0:T(8,128)(2,1)} %wo.1, f32[2]{0:T(128)} %lam.1, ...), custom_call_target="tpu_custom_call" | custom-call | tf_op jit(solution)/shard_map/pallas_call | solution.py:535
  113.1 1.9 %copy.12 = bf16[64,4096]{1,0:T(8,128)(2,1)} copy(bf16[64,4096]{1,0:T(8,128)(2,1)} %shard_map.100) | data formatting | bytes 1048576

commit v4 on v3

--- a/solution.py
+++ b/solution.py
@@ -350,18 +350,23 @@
         links.arrived(obuf.at[window(u * 256, 256), window(z * 256 + c * 128, 128)], sss.at[5], srs.at[c * 6 + 5])
     columns = TorusGather(links, opiece, oss, ors, obuf.at[pl.ds(0, 960), :])
     columns.begin()
+
+    def turned(i, rows):
+        v = proj[rows, i * QK : (i + 1) * QK]
+        swapped = jnp.concatenate([v[:, QK // 2 :], v[:, : QK // 2]], axis=1)
+        return (v * cos[rows] + swapped * sin[rows]).astype(BF)
+
+    def keep_keys(start, size):
+        rows = slice(start, start + size)
+        at = pl.ds(pl.multiple_of(place * ROWS + start, 128), size)
+        kvbuf[at, 0:QK] = turned(2, rows)
+        kvbuf[at, QK : 2 * QK] = turned(3, rows)
+        kvbuf[at, 2 * QK :] = proj[rows, 4 * QK :].astype(BF)
+
+    keep_keys(0, 384)
     far_tokens()
-    proj[384:512, :] = dot(tbuf[384:512, :], wbuf[...])
-
-    def turned(i):
-        v = proj[:, i * QK : (i + 1) * QK]
-        swapped = jnp.concatenate([v[:, QK // 2 :], v[:, : QK // 2]], axis=1)
-        return (v * cos[...] + swapped * sin[...]).astype(BF)
-
-    own_keys = window(place * ROWS, ROWS)
-    kvbuf[own_keys, 0:QK] = turned(2)
-    kvbuf[own_keys, QK : 2 * QK] = turned(3)
-    kvbuf[own_keys, 2 * QK :] = proj[:, 4 * QK :].astype(BF)
+    proj[384:512, 2 * QK :] = dot(tbuf[384:512, :], wbuf[:, 2 * QK :])
+    keep_keys(384, 128)
 
     def kpiece(dz, du, part, sub):
         start, size = ((0, 128), (128, 384))[part]
@@ -375,8 +380,9 @@
     crosses = jnp.logical_and(core == 1, crossed)
     plain(lown, lrecv, xss.at[0], xrs.at[0], "odd", only=crosses)
     pl.when(jnp.logical_not(crosses))(lambda: pltpu.make_async_copy(lown, lrecv, xrs.at[0]).start())
-    qbuf[0] = turned(0)
-    qbuf[1] = turned(1)
+    proj[384:512, 0 : 2 * QK] = dot(tbuf[384:512, :], wbuf[:, 0 : 2 * QK])
+    qbuf[0] = turned(0, slice(0, ROWS))
+    qbuf[1] = turned(1, slice(0, ROWS))
 
     def attend(index, at_u, masked, opening):
         span = window(index * ROWS, ROWS)

time: 115 us -> 115 us (level)
  no operation moved by 1% of the time
where the time goes in v4:
time: 115 us
  Pallas kernels  113 us (98%)
  local copies, waits for them, and re-layouts  1.87 us (2%)
    pallas_call x1, Pallas kernels, on_device(): pl.pallas_call(layer_kernel, out_shape=jax.ShapeDtypeStruct((64, 4096), B...  113 us

profile of v4, /device:TPU:1, one launch (start us, length us, event | category | flops | bytes accessed | tf_op | source)
XLA Modules:
  0.0 114.5 jit_solution(16565331065783358694)
XLA Ops:
  0.0 112.6 %shard_map.100 = bf16[64,4096]{1,0:T(8,128)(2,1)} custom-call(bf16[64,4096]{1,0:T(8,128)(2,1)} %tok.1, bf16[128,256]{1,0:T(8,128)(2,1)} %wq1.1, bf16[128,256]{1,0:T(8,128)(2,1)} %wq2.1, bf16[128,256]{1,0:T(8,128)(2,1)} %wk1.1, bf16[128,256]{1,0:T(8,128)(2,1)} %wk2.1, bf16[128,512]{1,0:T(8,128)(2,1)} %wv.1, bf16[512,128]{1,0:T(8,128)(2,1)} %wo.1, f32[2]{0:T(128)} %lam.1, ...), custom_call_target="tpu_custom_call" | custom-call | tf_op jit(solution)/shard_map/pallas_call | solution.py:541
  112.7 1.9 %copy.12 = bf16[64,4096]{1,0:T(8,128)(2,1)} copy(bf16[64,4096]{1,0:T(8,128)(2,1)} %shard_map.100) | data formatting | bytes 1048576

commit v5 on v4

--- a/solution.py
+++ b/solution.py
@@ -82,7 +82,7 @@
         return ("u", "z")[part ^ second]
 
     def out(self, part, key, dp, ds, sub, second, step):
-        k = part * 20 + key
+        k = part * 15 + key
 
         def views():
             view = self.ref(part, dp, ds, sub)
@@ -91,13 +91,13 @@
         self.links.send(views, self.axis(part, second), step, noted=False)
 
     def wait(self, part, key, dp, ds, sub):
-        k = part * 20 + key
+        k = part * 15 + key
         self.links.arrived(self.ref(part, dp, ds, sub), self.ssem.at[0], self.rsem.at[k])
 
     def spread(self, part, dp):
         i = NEAR.index(dp)
-        self.out(part, 4 + 4 * i, dp, 0, None, 1, 1)
-        self.out(part, 5 + 4 * i, dp, 0, None, 1, -1)
+        self.out(part, 3 + 3 * i, dp, 0, None, 1, 1)
+        self.out(part, 4 + 3 * i, dp, 0, None, 1, -1)
 
     def begin(self):
         for part in (0, 1):
@@ -111,32 +111,30 @@
             self.wait(part, 0, -1, 0, None)
             self.out(part, 2, -1, 0, 0, 0, 1)
             self.wait(part, 1, 1, 0, None)
-            self.out(part, 3, 1, 0, 1, 0, -1)
+            self.out(part, 2, 1, 0, 1, 0, -1)
         for part in (0, 1):
             self.spread(part, -1)
             self.spread(part, 1)
 
     def opposite(self):
         for part in (0, 1):
-            self.wait(part, 2, 2, 0, 0)
-            self.wait(part, 3, 2, 0, 1)
+            self.wait(part, 2, 2, 0, None)
             self.spread(part, 2)
 
     def second(self, dp, step):
         i = NEAR.index(dp)
         for part in (0, 1):
             if step < 0:
-                self.wait(part, 4 + 4 * i, dp, -1, None)
-                self.out(part, 6 + 4 * i, dp, -1, 0, 1, 1)
+                self.wait(part, 3 + 3 * i, dp, -1, None)
+                self.out(part, 5 + 3 * i, dp, -1, 0, 1, 1)
             else:
-                self.wait(part, 5 + 4 * i, dp, 1, None)
-                self.out(part, 7 + 4 * i, dp, 1, 1, 1, -1)
+                self.wait(part, 4 + 3 * i, dp, 1, None)
+                self.out(part, 5 + 3 * i, dp, 1, 1, 1, -1)
 
     def third(self, dp):
         i = NEAR.index(dp)
         for part in (0, 1):
-            self.wait(part, 6 + 4 * i, dp, 2, 0)
-            self.wait(part, 7 + 4 * i, dp, 2, 1)
+            self.wait(part, 5 + 3 * i, dp, 2, None)
 
     def steps(self):
         second, third = self.second, self.third
@@ -565,9 +563,9 @@
             pltpu.VMEM((8, 128), F32),
             pltpu.VMEM((8, 128), F32),
             dma((1,)),
-            dma((1,)), dma((40,)),
-            dma((1,)), dma((40,)),
-            dma((1,)), dma((40,)),
+            dma((1,)), dma((30,)),
+            dma((1,)), dma((30,)),
+            dma((1,)), dma((30,)),
             dma((7,)), dma((7,)),
             dma((12,)), dma((12,)),
             dma((17,)), dma((17,)),

time: 115 us -> 114 us (level)
  no operation moved by 1% of the time
where the time goes in v5:
time: 114 us
  Pallas kernels  112 us (98%)
  local copies, waits for them, and re-layouts  1.87 us (2%)
    pallas_call x1, Pallas kernels, on_device(): pl.pallas_call(layer_kernel, out_shape=jax.ShapeDtypeStruct((64, 4096), B...  112 us

profile of v5, /device:TPU:1, one launch (start us, length us, event | category | flops | bytes accessed | tf_op | source)
XLA Modules:
  0.0 114.3 jit_solution(3149795563770349038)
XLA Ops:
  0.0 112.4 %shard_map.100 = bf16[64,4096]{1,0:T(8,128)(2,1)} custom-call(bf16[64,4096]{1,0:T(8,128)(2,1)} %tok.1, bf16[128,256]{1,0:T(8,128)(2,1)} %wq1.1, bf16[128,256]{1,0:T(8,128)(2,1)} %wq2.1, bf16[128,256]{1,0:T(8,128)(2,1)} %wk1.1, bf16[128,256]{1,0:T(8,128)(2,1)} %wk2.1, bf16[128,512]{1,0:T(8,128)(2,1)} %wv.1, bf16[512,128]{1,0:T(8,128)(2,1)} %wo.1, f32[2]{0:T(128)} %lam.1, ...), custom_call_target="tpu_custom_call" | custom-call | tf_op jit(solution)/shard_map/pallas_call | solution.py:539
  112.4 1.9 %copy.12 = bf16[64,4096]{1,0:T(8,128)(2,1)} copy(bf16[64,4096]{1,0:T(8,128)(2,1)} %shard_map.100) | data formatting | bytes 1048576
